TPU v7x, 32 devices: a whole 2x2x4 slice. The times are simulated.
32 devices in a mesh: kv: 8 (over z, core), tp: 4 (over y, x).
Axes of the slice: x: 2, y: 2, z: 4, core: 2. Of those that a mesh axis runs over, the one named last changes fastest.
Arguments:
- tokens: bfloat16 [16, 2048], P(None, 'kv'), may hold values from -8 to 8
- lengths: int32 [16], replicated, may hold values from 1 to 3072, 12288 in all
- latent_cache: bfloat16 [16, 3072, 256], P(None, ('kv', 'tp')), may hold values from -10 to 10
- rope_cache: bfloat16 [16, 3072, 32], P(None, ('kv', 'tp')), may hold values from -2000 to 2000
- gain_in: bfloat16 [2048], P('kv'), may hold values from 0.099609375 to 1.8984375
- w_down_q: bfloat16 [2048, 512], P('kv'), may hold values from -0.125 to 0.125
- w_down_kv: bfloat16 [2048, 256], P('kv'), may hold values from -0.125 to 0.125
- w_rope_key: bfloat16 [2048, 32], P('kv'), may hold values from -0.125 to 0.125
- gain_q: bfloat16 [512], replicated, may hold values from 0.099609375 to 1.8984375
- w_up_qn: bfloat16 [512, 16, 64], replicated, may hold values from -0.25 to 0.25
- w_up_qr: bfloat16 [512, 16, 32], replicated, may hold values from -0.25 to 0.25
- gain_kv: bfloat16 [256], replicated, may hold values from 0.099609375 to 1.8984375
- w_key_up: bfloat16 [256, 16, 64], replicated, may hold values from -0.375 to 0.375
- w_value_up: bfloat16 [256, 16, 64], replicated, may hold values from -0.375 to 0.375
- w_attn_out: bfloat16 [16, 64, 2048], P('tp', None, 'kv'), may hold values from -0.1875 to 0.1875
- gain_mid: bfloat16 [2048], P('kv'), may hold values from 0.099609375 to 1.8984375
- w_ff_in: bfloat16 [2048, 8192], P('kv', 'tp'), may hold values from -0.125 to 0.125
- w_ff_out: bfloat16 [8192, 2048], P('tp', 'kv'), may hold values from -0.0625 to 0.0625
Outputs:
- mixed: bfloat16 [16, 2048], P(None, 'kv')
- new_latent: bfloat16 [16, 256], replicated
- new_rope_key: bfloat16 [16, 32], replicated
Inputs may be any that keep to these rules, and one draw needn't show every extreme that they name: `lengths`: each sequence's live cache positions; one sequence fills the whole cache.
All inputs are finite; a program needn't handle non-finite values.
Results may differ from a plain program's by a relative error of at most 0.012.
Values sent between devices are 32-bit elements; how exact they have to be, the bound alone decides.
No kernel may reach another device: no remote copies, remote signals or barrier semaphores. Data moves between devices by JAX's collectives and lax.ppermute only.
A program may use at most 64 MiB of HBM per device.

v0:
```python
import jax
import jax.numpy as jnp
from jax import lax
from jax.sharding import PartitionSpec as P

D = 2048
NOPE = 64
ROPE = 32
EPS = 1e-06


def combined_all(part, axis, combine):
    gathered = jax.tree.map(lambda a: lax.all_gather(a, axis), part)

    def take(source):
        return jax.tree.map(lambda a: lax.dynamic_index_in_dim(a, source, 0, False), gathered)

    return lax.fori_loop(
        1, lax.axis_size(axis), lambda source, state: combine(state, take(source)), take(0)
    )


def rotate(values, positions):
    half = values.shape[-1] // 2
    inverse = 10000.0 ** (-jnp.arange(half, dtype=jnp.float32) / half)
    angle = positions.astype(jnp.float32)[:, None, None] * inverse[None, None, :]
    first = values[..., :half]
    second = values[..., half:]
    return jnp.concatenate(
        [
            first * jnp.cos(angle) - second * jnp.sin(angle),
            second * jnp.cos(angle) + first * jnp.sin(angle),
        ],
        axis=-1,
    )


def rms_scaled(values, gain):
    return (
        values
        * lax.rsqrt(jnp.mean(values * values, axis=-1, keepdims=True) + EPS)
        * gain.astype(jnp.float32)
    )


def combine(earlier, later):
    top_a, total_a, acc_a = earlier
    top_b, total_b, acc_b = later
    top = jnp.maximum(top_a, top_b)
    fade_a = jnp.exp(top_a - top)
    fade_b = jnp.exp(top_b - top)
    return (
        top,
        total_a * fade_a + total_b * fade_b,
        acc_a * fade_a[..., None] + acc_b * fade_b[..., None],
    )


def fold_sources(parts):
    tops, totals, accs = parts
    top = jnp.max(tops, axis=0)
    fade = jnp.exp(tops - top[None])
    return (top, jnp.sum(totals * fade, axis=0), jnp.sum(accs * fade[..., None], axis=0))


def per_device(
    tokens,
    lengths,
    latent_cache,
    rope_cache,
    gain_in,
    w_down_q,
    w_down_kv,
    w_rope_key,
    gain_q,
    w_up_qn,
    w_up_qr,
    gain_kv,
    w_key_up,
    w_value_up,
    w_attn_out,
    gain_mid,
    w_ff_in,
    w_ff_out,
):
    f32 = jnp.float32
    bf16 = jnp.bfloat16
    highest = lax.Precision.HIGHEST
    scale = (NOPE + ROPE) ** (-0.5)
    resid = tokens.astype(f32)
    scaled_in = (resid * gain_in.astype(f32)).astype(bf16)
    part_q = jnp.dot(scaled_in, w_down_q, preferred_element_type=f32)
    part_kv = jnp.dot(scaled_in, w_down_kv, preferred_element_type=f32)
    part_rope = jnp.dot(scaled_in, w_rope_key, preferred_element_type=f32)
    square_in = jnp.sum(resid * resid, axis=1)
    sum_q, sum_kv, sum_rope, total_in = lax.psum((part_q, part_kv, part_rope, square_in), "kv")
    inv_in = lax.rsqrt(total_in / D + EPS)[:, None]
    query_latent = rms_scaled(inv_in * sum_q, gain_q).astype(bf16)
    new_latent = rms_scaled(inv_in * sum_kv, gain_kv).astype(bf16)
    new_rope_key = rotate((inv_in * sum_rope)[:, None, :], lengths)[:, 0, :].astype(bf16)
    query_nope = jnp.einsum(
        "bc,chd->bhd", query_latent, w_up_qn, preferred_element_type=f32
    ).astype(bf16)
    query_rope = rotate(
        jnp.einsum("bc,chr->bhr", query_latent, w_up_qr, preferred_element_type=f32), lengths
    ).astype(bf16)
    query_cache = jnp.einsum(
        "bhd,khd->bhk", query_nope, w_key_up, preferred_element_type=f32
    ).astype(bf16)
    rows = latent_cache.shape[1]
    positions = lax.axis_index(("kv", "tp")) * rows + jnp.arange(rows, dtype=jnp.int32)
    live = (positions[None, :] < lengths[:, None])[:, None, :]
    scores = (
        jnp.einsum("bhk,blk->bhl", query_cache, latent_cache, preferred_element_type=f32)
        + jnp.einsum("bhr,blr->bhl", query_rope, rope_cache, preferred_element_type=f32)
    ) * scale
    scores = jnp.where(live, scores, -1e30)
    top = jnp.max(scores, axis=2)
    weights = jnp.where(live, jnp.exp(scores - top[:, :, None]), 0.0)
    total = jnp.sum(weights, axis=2)
    acc = jnp.einsum("bhl,blk->bhk", weights.astype(bf16), latent_cache, preferred_element_type=f32)
    heads_dev = w_attn_out.shape[0]
    first_head = lax.axis_index("tp") * heads_dev
    own_value_up = lax.dynamic_slice_in_dim(w_value_up, first_head, heads_dev, 1).astype(f32)
    own_cache_q = lax.dynamic_slice_in_dim(query_cache, first_head, heads_dev, 1)
    own_rope_q = lax.dynamic_slice_in_dim(query_rope, first_head, heads_dev, 1)
    self_score = (
        jnp.einsum("bhk,bk->bh", own_cache_q, new_latent, preferred_element_type=f32)
        + jnp.einsum("bhr,br->bh", own_rope_q, new_rope_key, preferred_element_type=f32)
    ) * scale
    top, total, acc = fold_sources(
        (
            lax.all_to_all(top[None], "tp", split_axis=2, concat_axis=0, tiled=True),
            lax.all_to_all(total[None], "tp", split_axis=2, concat_axis=0, tiled=True),
            lax.all_to_all(acc[None], "tp", split_axis=2, concat_axis=0, tiled=True),
        )
    )
    top, total, acc = combined_all((top, total, acc), "kv", combine)
    joined = jnp.maximum(top, self_score)
    fade = jnp.exp(top - joined)
    self_weight = jnp.exp(self_score - joined)
    total = total * fade + self_weight
    acc = (
        acc * fade[:, :, None]
        + self_weight.astype(bf16).astype(f32)[:, :, None] * new_latent.astype(f32)[:, None, :]
    )
    expanded = jnp.einsum("bhk,khv->bhv", acc, own_value_up, precision=highest)
    head_out = (expanded / total[:, :, None]).astype(bf16)
    attn_part = jnp.einsum("bhv,hvd->bd", head_out, w_attn_out, preferred_element_type=f32)
    resid_mid = resid + lax.psum(attn_part, "tp")
    scaled_mid = (resid_mid * gain_mid.astype(f32)).astype(bf16)
    hidden_part = jnp.dot(scaled_mid, w_ff_in, preferred_element_type=f32)
    square_mid = jnp.sum(resid_mid * resid_mid, axis=1)
    hidden_sum, total_mid = lax.psum((hidden_part, square_mid), "kv")
    inv_mid = lax.rsqrt(total_mid / D + EPS)[:, None]
    hidden = jnp.square(jax.nn.relu(inv_mid * hidden_sum)).astype(bf16)
    out_part = jnp.dot(hidden, w_ff_out, preferred_element_type=f32)
    mixed = (resid_mid + lax.psum(out_part, "tp")).astype(bf16)
    return (mixed, new_latent, new_rope_key)


def solution(mesh):
    return jax.shard_map(
        per_device,
        mesh=mesh,
        in_specs=(
            P(None, "kv"),
            P(),
            P(None, ("kv", "tp"), None),
            P(None, ("kv", "tp"), None),
            P("kv"),
            P("kv", None),
            P("kv", None),
            P("kv", None),
            P(),
            P(),
            P(),
            P(),
            P(),
            P(),
            P("tp", None, "kv"),
            P("kv"),
            P("kv", "tp"),
            P("tp", "kv"),
        ),
        out_specs=(P(None, "kv"), P(), P()),
        check_vma=False,
    )
```

profile of v0, /device:TPU:0, one launch (start us, length us, event | category | flops | bytes accessed | tf_op | source)
XLA Modules:
  0.0 218.2 jit_solution(16655276583001931939)
XLA Ops:
  7.2 0.8 convert_element_type.75
  8.0 0.8 fusion.23
  8.8 0.7 convert_element_type.68
  9.5 0.7 broadcast_compare_fusion
  10.2 0.7 convert_element_type.70
  10.9 0.9 fusion.41
  11.7 1.1 fusion.43
  12.8 1.2 fusion.45
  14.0 30.8 %all-reduce = (f32[16,512]{1,0:T(8,128)S(1)}, f32[16]{0:T(128)S(1)}, f32[16,256]{1,0:T(8,128)S(1)}, f32[16,32]{1,0:T(8,128)S(1)}) all-reduce(f32[16,512]{1,0:T(8,128)S(1)} %fusion.45, f32[16]{0:T(128)S(1)} %fusion.23, f32[16,256]{1,0:T(8,128)S(1)} %fusion.43, f32[16,32]{1,0:T(8,128)S(1)} %fusion.41), channel_id=1, replica_groups=mesh['kv'=8,'tp'=4] {'kv'}, use_global_device_ids=true, to_apply=%region_2.0 | all-reduce | flops 12816 | bytes 102528 | tf_op jit(solution)/shard_map/psum | solution.py:96
  44.8 0.2 multiply_reduce_fusion.1
  45.1 0.5 fusion.55
  45.6 0.7 convolution_convert_fusion
  46.5 0.1 fusion.14
  46.7 0.8 copy-done.1
  47.4 0.4 fusion.62
  47.8 0.7 copy.50
  48.5 3.7 %all-to-all-start = ((f32[1,16,16]{1,0,2:T(1,128)}), f32[1,16,16]{1,0,2:T(1,128)S(1)}, u32[]{:S(2)}, u32[]{:S(2)}) async-start(f32[1,16,16]{1,0,2:T(1,128)} %copy.50), calls=%async_computation | async-start | bytes 16384 | tf_op jit(solution)/shard_map/all_to_all | solution.py:133
  52.3 0.6 copy-done.10
  53.1 0.2 multiply_reduce_fusion.3
  53.3 0.3 convolution_bitcast_fusion
  53.6 0.7 fusion.52
  54.5 0.5 copy-done.9
  55.0 0.2 fusion.10
  55.3 0.6 copy-done.11
  56.1 0.7 copy.51
  56.8 0.8 copy.52
  57.6 4.2 %all-to-all-start.1 = ((f32[1,16,16]{1,0,2:T(1,128)}), f32[1,16,16]{1,0,2:T(1,128)S(1)}, u32[]{:S(2)}, u32[]{:S(2)}) async-start(f32[1,16,16]{1,0,2:T(1,128)} %copy.51), calls=%async_computation.1 | async-start | bytes 16384 | tf_op jit(solution)/shard_map/all_to_all | solution.py:134
  61.8 12.8 %all-gather.3 = f32[8,16,4]{1,2,0:T(4,128)S(1)} all-gather(f32[1,16,4]{1,2,0:T(4,128)S(1)} %bitcast.113), channel_id=2, replica_groups=mesh['kv'=8,'tp'=4] {'kv'}, dimensions={0}, use_global_device_ids=true | all-gather | bytes 2304 | tf_op jit(solution)/shard_map/all_gather | solution.py:13
  74.6 4.2 %all-to-all-start.2 = ((f32[1,16,16,256]{3,1,0,2:T(8,128)}), f32[1,16,16,256]{3,1,0,2:T(8,128)S(1)}, u32[]{:S(2)}, u32[]{:S(2)}) async-start(f32[1,16,16,256]{3,1,0,2:T(8,128)} %copy.52), calls=%async_computation.2 | async-start | bytes 524288 | tf_op jit(solution)/shard_map/all_to_all | solution.py:135
  78.8 12.8 %all-gather.4 = f32[8,16,4]{1,2,0:T(4,128)S(1)} all-gather(f32[1,16,4]{1,2,0:T(4,128)S(1)} %bitcast.114), channel_id=3, replica_groups=mesh['kv'=8,'tp'=4] {'kv'}, dimensions={0}, use_global_device_ids=true | all-gather | bytes 2304 | tf_op jit(solution)/shard_map/all_gather | solution.py:13
  91.8 15.1 %all-gather.2 = f32[128,4,256]{2,1,0:T(4,128)S(1)} all-gather(f32[16,4,256]{2,1,0:T(4,128)S(1)} %copy.53), channel_id=4, replica_groups=mesh['kv'=8,'tp'=4] {'kv'}, dimensions={0}, use_global_device_ids=true | all-gather | bytes 589824 | tf_op jit(solution)/shard_map/all_gather | solution.py:13
  106.8 2.5 %while.19 = (s32[]{:T(128)}, f32[16,4]{0,1:T(4,128)S(1)}, f32[16,4]{0,1:T(4,128)S(1)}, f32[16,4,256]{2,1,0:T(4,128)S(1)}, f32[8,16,4]{1,2,0:T(4,128)S(1)}, /*ind...) while((s32[]{:T(128)}, f32[16,4]{0,1:T(4,128)S(1)}, ...), condition=%wide.region_10.11_spmd, body=%wide.region_9.10_spmd.sunk | while | flops 49541 | bytes 200335 | solution.py:18
  107.0 0.1 fusion.79
  107.4 0.1 fusion.79
  107.8 0.1 fusion.79
  108.1 0.1 fusion.79
  108.5 0.1 fusion.79
  108.8 0.1 fusion.79
  109.2 0.1 fusion.79
  109.6 1.2 fusion.6
  110.8 0.2 convolution_bitcast_fusion.2
  111.0 16.5 %psum.60 = f32[16,256]{1,0:T(8,128)S(1)} all-reduce(f32[16,256]{1,0:T(8,128)S(1)} %convolution_bitcast_fusion.2), channel_id=1, replica_groups=mesh['kv'=8,'tp'=4] {'tp'}, use_global_device_ids=true, to_apply=%region_14.15 | all-reduce | flops 4096 | bytes 32768 | tf_op jit(solution)/shard_map/psum | solution.py:150
  127.6 13.6 %psum.61 = f32[16]{0:T(128)S(1)} all-reduce(f32[16]{0:T(128)S(1)} %multiply_reduce_fusion.2), channel_id=1, replica_groups=mesh['kv'=8,'tp'=4] {'kv'}, use_global_device_ids=true, to_apply=%region_16.17 | all-reduce | flops 16 | bytes 128 | tf_op jit(solution)/shard_map/psum | solution.py:154
  141.2 0.9 fusion.38
  142.2 51.4 %all-reduce.3.cloned.1.call-done = f32[16,2048]{1,0:T(8,128)} async-done(((f32[16,2048]{1,0:T(8,128)}), f32[16,2048]{1,0:T(8,128)}) %all-reduce.3.cloned.1.call-update) | async-done | bytes 131088 | tf_op jit(solution)/shard_map/psum | solution.py:154
  193.6 1.2 fusion.12
  194.8 16.0 %psum.63 = f32[16,256]{1,0:T(8,128)S(1)} all-reduce(f32[16,256]{1,0:T(8,128)S(1)} %fusion.12), channel_id=1, replica_groups=mesh['kv'=8,'tp'=4] {'tp'}, use_global_device_ids=true, to_apply=%region_18.19 | all-reduce | flops 4096 | bytes 32768 | tf_op jit(solution)/shard_map/psum | solution.py:158
  210.7 0.6 add_convert_fusion.1
  (78 shorter events, 3.2 us)
Async XLA Ops:
  7.2 38.4 %copy-start = (bf16[512,16,64]{0,2,1:T(8,128)(2,1)S(1)}, bf16[512,16,64]{0,2,1:T(8,128)(2,1)}, u32[]{:S(2)}) copy-start(bf16[512,16,64]{0,2,1:T(8,128)(2,1)} %param.29) | copy-start | bytes 3145732
  7.2 37.9 %copy-start.4 = (bf16[512,16,32]{0,2,1:T(8,128)(2,1)S(1)}, bf16[512,16,32]{0,2,1:T(8,128)(2,1)}, u32[]{:S(2)}) copy-start(bf16[512,16,32]{0,2,1:T(8,128)(2,1)} %param.30) | copy-start | bytes 1572868
  12.8 32.8 %copy-start.5 = (bf16[256,16,64]{0,2,1:T(8,128)(2,1)S(1)}, bf16[256,16,64]{0,2,1:T(8,128)(2,1)}, u32[]{:S(2)}) copy-start(bf16[256,16,64]{0,2,1:T(8,128)(2,1)} %param.32) | copy-start | bytes 1572868
  45.6 0.9 copy-start.8
  46.3 1.2 copy-start.1
  48.5 9.1 %all-to-all-start = ((f32[1,16,16]{1,0,2:T(1,128)}), f32[1,16,16]{1,0,2:T(1,128)S(1)}, u32[]{:S(2)}, u32[]{:S(2)}) async-start(f32[1,16,16]{1,0,2:T(1,128)} %copy.50), calls=%async_computation | async-start | bytes 16384 | tf_op jit(solution)/shard_map/all_to_all | solution.py:133
  52.2 0.7 copy-start.10
  54.3 0.6 copy-start.9
  55.3 0.7 copy-start.11
  57.6 17.0 %all-to-all-start.1 = ((f32[1,16,16]{1,0,2:T(1,128)}), f32[1,16,16]{1,0,2:T(1,128)S(1)}, u32[]{:S(2)}, u32[]{:S(2)}) async-start(f32[1,16,16]{1,0,2:T(1,128)} %copy.51), calls=%async_computation.1 | async-start | bytes 16384 | tf_op jit(solution)/shard_map/all_to_all | solution.py:134
  74.6 17.0 %all-to-all-start.2 = ((f32[1,16,16,256]{3,1,0,2:T(8,128)}), f32[1,16,16,256]{3,1,0,2:T(8,128)S(1)}, u32[]{:S(2)}, u32[]{:S(2)}) async-start(f32[1,16,16,256]{3,1,0,2:T(8,128)} %copy.52), calls=%async_computation.2 | async-start | bytes 524288 | tf_op jit(solution)/shard_map/all_to_all | solution.py:135
  78.8 114.8 %all-reduce.3.cloned.1.call-start = ((), (), s32[]{:S(2)}) async-start(), calls=%async_computation.3 | async-start | bytes 262144 | tf_op jit(solution)/shard_map/psum | solution.py:154
  91.7 19.0 %copy-start.7 = (bf16[4,64,256]{2,1,0:T(8,128)(2,1)S(1)}, bf16[4,64,256]{2,1,0:T(8,128)(2,1)}, u32[]{:S(2)}) copy-start(bf16[4,64,256]{2,1,0:T(8,128)(2,1)} %param.34) | copy-start | bytes 393220
  106.8 34.4 %copy-start.2 = (bf16[256,2048]{1,0:T(8,128)(2,1)S(1)}, bf16[256,2048]{1,0:T(8,128)(2,1)}, u32[]{:S(2)}) copy-start(bf16[256,2048]{1,0:T(8,128)(2,1)} %param.36) | copy-start | bytes 3145732
  106.8 20.7 %copy-start.6 = (bf16[16,256]{1,0:T(8,128)(2,1)S(1)}, bf16[16,256]{1,0:T(8,128)(2,1)}, u32[]{:S(2)}) copy-start(bf16[16,256]{1,0:T(8,128)(2,1)} %param.20) | copy-start | bytes 24580
  109.3 84.3 %copy-start.3 = (bf16[2048,256]{1,0:T(8,128)(2,1)S(1)}, bf16[2048,256]{1,0:T(8,128)(2,1)}, u32[]{:S(2)}) copy-start(bf16[2048,256]{1,0:T(8,128)(2,1)} %param.37) | copy-start | bytes 3145732
Sparse Core Ops, SparseCore 0:
  142.3 51.2 all-reduce.2
where the time goes:
time: 219 us; the launch traced here: 218 us
  blocking collectives  117 us (53%)
  waiting for transfers between devices  51.5 us (24%)
  between operations  14.2 us (6%)
  starting transfers between devices  12.1 us (6%)
  matrix products  8.74 us (4%)
  other arithmetic  7.81 us (4%)
  local copies, waits for them, and re-layouts  6.26 us (3%)
    psum x1, waiting for transfers between devices, per_device(): hidden_sum, total_mid = lax.psum((hidden_part, square_mid), 'kv')  51.4 us
    all_gather x3, blocking collectives, combined_all(): gathered = jax.tree.map(lambda a: lax.all_gather(a, axis), part)  40.6 us
    psum x1, blocking collectives, per_device(): lax.psum((part_q, part_kv, part_rope, square_in), 'kv')  30.8 us
    psum x1, blocking collectives, per_device(): resid_mid = resid + lax.psum(attn_part, 'tp')  16.5 us
    psum x1, blocking collectives, per_device(): mixed = (resid_mid + lax.psum(out_part, 'tp')).astype(bf16)  16 us
    psum x1, blocking collectives, per_device(): hidden_sum, total_mid = lax.psum((hidden_part, square_mid), 'kv')  13.6 us
  transfers between devices with their start and end apart: 4, of which 1 were waited for; matrix products, arithmetic and copies ran while one was open for 2% of the time, Pallas kernels for 0%

commit v1 on v0

--- a/solution.py
+++ b/solution.py
@@ -7,6 +7,11 @@
 NOPE = 64
 ROPE = 32
 EPS = 1e-06
+
+
+def gather_and_add(value, axis):
+    blocks = lax.all_gather(value, axis)
+    return jnp.sum(blocks, axis=0)
 
 
 def combined_all(part, axis, combine):
@@ -155,7 +160,7 @@
     inv_mid = lax.rsqrt(total_mid / D + EPS)[:, None]
     hidden = jnp.square(jax.nn.relu(inv_mid * hidden_sum)).astype(bf16)
     out_part = jnp.dot(hidden, w_ff_out, preferred_element_type=f32)
-    mixed = (resid_mid + lax.psum(out_part, "tp")).astype(bf16)
+    mixed = (resid_mid + gather_and_add(out_part, "tp")).astype(bf16)
     return (mixed, new_latent, new_rope_key)
 
 

time: 219 us -> 211 us (0.963)
  blocking collectives: 117 us -> 110 us
    psum x1 -> x0, blocking collectives: 16 us -> none  [per_device(): mixed = (resid_mid + lax.psum(out_part, 'tp')).astype(bf16)]
    all_gather x0 -> x1, blocking collectives: none -> 8.19 us  [gather_and_add(): blocks = lax.all_gather(value, axis)]
where the time goes in v1:
time: 211 us; the launch traced here: 210 us
  blocking collectives  110 us (52%)
  waiting for transfers between devices  51.5 us (24%)
  between operations  14.3 us (7%)
  starting transfers between devices  12.1 us (6%)
  matrix products  8.74 us (4%)
  other arithmetic  7.82 us (4%)
  local copies, waits for them, and re-layouts  6.26 us (3%)
    psum x1, waiting for transfers between devices, per_device(): hidden_sum, total_mid = lax.psum((hidden_part, square_mid), 'kv')  51.4 us
    all_gather x3, blocking collectives, combined_all(): gathered = jax.tree.map(lambda a: lax.all_gather(a, axis), part)  40.6 us
    psum x1, blocking collectives, per_device(): lax.psum((part_q, part_kv, part_rope, square_in), 'kv')  30.8 us
    psum x1, blocking collectives, per_device(): resid_mid = resid + lax.psum(attn_part, 'tp')  16.5 us
    psum x1, blocking collectives, per_device(): hidden_sum, total_mid = lax.psum((hidden_part, square_mid), 'kv')  13.6 us
    all_gather x1, blocking collectives, gather_and_add(): blocks = lax.all_gather(value, axis)  8.19 us
  transfers between devices with their start and end apart: 4, of which 1 were waited for; matrix products, arithmetic and copies ran while one was open for 2% of the time, Pallas kernels for 0%

profile of v1, /device:TPU:0, one launch (start us, length us, event | category | flops | bytes accessed | tf_op | source)
XLA Modules:
  0.0 210.4 jit_solution(328475554746534807)
XLA Ops:
  7.2 0.8 convert_element_type.75
  8.0 0.8 fusion.23
  8.8 0.7 convert_element_type.68
  9.5 0.7 broadcast_compare_fusion
  10.2 0.7 convert_element_type.70
  10.9 0.9 fusion.41
  11.7 1.1 fusion.43
  12.8 1.2 fusion.45
  14.0 30.8 %all-reduce = (f32[16,512]{1,0:T(8,128)S(1)}, f32[16]{0:T(128)S(1)}, f32[16,256]{1,0:T(8,128)S(1)}, f32[16,32]{1,0:T(8,128)S(1)}) all-reduce(f32[16,512]{1,0:T(8,128)S(1)} %fusion.45, f32[16]{0:T(128)S(1)} %fusion.23, f32[16,256]{1,0:T(8,128)S(1)} %fusion.43, f32[16,32]{1,0:T(8,128)S(1)} %fusion.41), channel_id=1, replica_groups=mesh['kv'=8,'tp'=4] {'kv'}, use_global_device_ids=true, to_apply=%region_2.0 | all-reduce | flops 12816 | bytes 102528 | tf_op jit(solution)/shard_map/psum | solution.py:101
  44.8 0.2 multiply_reduce_fusion.1
  45.1 0.5 fusion.55
  45.6 0.7 convolution_convert_fusion
  46.5 0.1 fusion.14
  46.7 0.8 copy-done.1
  47.4 0.4 fusion.62
  47.8 0.7 copy.50
  48.5 3.7 %all-to-all-start = ((f32[1,16,16]{1,0,2:T(1,128)}), f32[1,16,16]{1,0,2:T(1,128)S(1)}, u32[]{:S(2)}, u32[]{:S(2)}) async-start(f32[1,16,16]{1,0,2:T(1,128)} %copy.50), calls=%async_computation | async-start | bytes 16384 | tf_op jit(solution)/shard_map/all_to_all | solution.py:138
  52.3 0.6 copy-done.10
  53.1 0.2 multiply_reduce_fusion.3
  53.3 0.3 convolution_bitcast_fusion
  53.6 0.7 fusion.52
  54.5 0.5 copy-done.9
  55.0 0.2 fusion.10
  55.3 0.6 copy-done.11
  56.1 0.7 copy.51
  56.8 0.8 copy.52
  57.6 4.2 %all-to-all-start.1 = ((f32[1,16,16]{1,0,2:T(1,128)}), f32[1,16,16]{1,0,2:T(1,128)S(1)}, u32[]{:S(2)}, u32[]{:S(2)}) async-start(f32[1,16,16]{1,0,2:T(1,128)} %copy.51), calls=%async_computation.1 | async-start | bytes 16384 | tf_op jit(solution)/shard_map/all_to_all | solution.py:139
  61.8 12.8 %all-gather.4 = f32[8,16,4]{1,2,0:T(4,128)S(1)} all-gather(f32[1,16,4]{1,2,0:T(4,128)S(1)} %bitcast.115), channel_id=2, replica_groups=mesh['kv'=8,'tp'=4] {'kv'}, dimensions={0}, use_global_device_ids=true | all-gather | bytes 2304 | tf_op jit(solution)/shard_map/all_gather | solution.py:18
  74.6 4.2 %all-to-all-start.2 = ((f32[1,16,16,256]{3,1,0,2:T(8,128)}), f32[1,16,16,256]{3,1,0,2:T(8,128)S(1)}, u32[]{:S(2)}, u32[]{:S(2)}) async-start(f32[1,16,16,256]{3,1,0,2:T(8,128)} %copy.52), calls=%async_computation.2 | async-start | bytes 524288 | tf_op jit(solution)/shard_map/all_to_all | solution.py:140
  78.8 12.8 %all-gather.5 = f32[8,16,4]{1,2,0:T(4,128)S(1)} all-gather(f32[1,16,4]{1,2,0:T(4,128)S(1)} %bitcast.116), channel_id=3, replica_groups=mesh['kv'=8,'tp'=4] {'kv'}, dimensions={0}, use_global_device_ids=true | all-gather | bytes 2304 | tf_op jit(solution)/shard_map/all_gather | solution.py:18
  91.8 15.1 %all-gather.2 = f32[128,4,256]{2,1,0:T(4,128)S(1)} all-gather(f32[16,4,256]{2,1,0:T(4,128)S(1)} %copy.53), channel_id=4, replica_groups=mesh['kv'=8,'tp'=4] {'kv'}, dimensions={0}, use_global_device_ids=true | all-gather | bytes 589824 | tf_op jit(solution)/shard_map/all_gather | solution.py:18
  106.8 2.5 %while.19 = (s32[]{:T(128)}, f32[16,4]{0,1:T(4,128)S(1)}, f32[16,4]{0,1:T(4,128)S(1)}, f32[16,4,256]{2,1,0:T(4,128)S(1)}, f32[8,16,4]{1,2,0:T(4,128)S(1)}, /*ind...) while((s32[]{:T(128)}, f32[16,4]{0,1:T(4,128)S(1)}, ...), condition=%wide.region_10.11_spmd, body=%wide.region_9.10_spmd.sunk | while | flops 49541 | bytes 200335 | solution.py:23
  107.0 0.1 fusion.79
  107.4 0.1 fusion.79
  107.8 0.1 fusion.79
  108.1 0.1 fusion.79
  108.5 0.1 fusion.79
  108.8 0.1 fusion.79
  109.2 0.1 fusion.79
  109.6 1.2 fusion.6
  110.8 0.2 convolution_bitcast_fusion.2
  111.0 16.5 %psum.53 = f32[16,256]{1,0:T(8,128)S(1)} all-reduce(f32[16,256]{1,0:T(8,128)S(1)} %convolution_bitcast_fusion.2), channel_id=1, replica_groups=mesh['kv'=8,'tp'=4] {'tp'}, use_global_device_ids=true, to_apply=%region_14.15 | all-reduce | flops 4096 | bytes 32768 | tf_op jit(solution)/shard_map/psum | solution.py:155
  127.6 13.6 %psum.54 = f32[16]{0:T(128)S(1)} all-reduce(f32[16]{0:T(128)S(1)} %multiply_reduce_fusion.2), channel_id=1, replica_groups=mesh['kv'=8,'tp'=4] {'kv'}, use_global_device_ids=true, to_apply=%region_16.17 | all-reduce | flops 16 | bytes 128 | tf_op jit(solution)/shard_map/psum | solution.py:159
  141.2 0.9 fusion.38
  142.2 51.4 %all-reduce.3.cloned.1.call-done = f32[16,2048]{1,0:T(8,128)} async-done(((f32[16,2048]{1,0:T(8,128)}), f32[16,2048]{1,0:T(8,128)}) %all-reduce.3.cloned.1.call-update) | async-done | bytes 131088 | tf_op jit(solution)/shard_map/psum | solution.py:159
  193.6 1.2 fusion.12
  194.8 8.2 %all-gather.3 = f32[64,256]{1,0:T(8,128)S(1)} all-gather(f32[16,256]{1,0:T(8,128)S(1)} %fusion.12), channel_id=5, replica_groups=mesh['kv'=8,'tp'=4] {'tp'}, dimensions={0}, use_global_device_ids=true | all-gather | bytes 81920 | tf_op jit(solution)/shard_map/all_gather | solution.py:13
  203.0 0.6 add_convert_fusion.1
  (79 shorter events, 3.2 us)
Async XLA Ops:
  7.2 38.4 %copy-start = (bf16[512,16,64]{0,2,1:T(8,128)(2,1)S(1)}, bf16[512,16,64]{0,2,1:T(8,128)(2,1)}, u32[]{:S(2)}) copy-start(bf16[512,16,64]{0,2,1:T(8,128)(2,1)} %param.29) | copy-start | bytes 3145732
  7.2 37.9 %copy-start.4 = (bf16[512,16,32]{0,2,1:T(8,128)(2,1)S(1)}, bf16[512,16,32]{0,2,1:T(8,128)(2,1)}, u32[]{:S(2)}) copy-start(bf16[512,16,32]{0,2,1:T(8,128)(2,1)} %param.30) | copy-start | bytes 1572868
  12.8 32.8 %copy-start.5 = (bf16[256,16,64]{0,2,1:T(8,128)(2,1)S(1)}, bf16[256,16,64]{0,2,1:T(8,128)(2,1)}, u32[]{:S(2)}) copy-start(bf16[256,16,64]{0,2,1:T(8,128)(2,1)} %param.32) | copy-start | bytes 1572868
  45.6 0.9 copy-start.8
  46.3 1.2 copy-start.1
  48.5 9.1 %all-to-all-start = ((f32[1,16,16]{1,0,2:T(1,128)}), f32[1,16,16]{1,0,2:T(1,128)S(1)}, u32[]{:S(2)}, u32[]{:S(2)}) async-start(f32[1,16,16]{1,0,2:T(1,128)} %copy.50), calls=%async_computation | async-start | bytes 16384 | tf_op jit(solution)/shard_map/all_to_all | solution.py:138
  52.2 0.7 copy-start.10
  54.3 0.6 copy-start.9
  55.3 0.7 copy-start.11
  57.6 17.0 %all-to-all-start.1 = ((f32[1,16,16]{1,0,2:T(1,128)}), f32[1,16,16]{1,0,2:T(1,128)S(1)}, u32[]{:S(2)}, u32[]{:S(2)}) async-start(f32[1,16,16]{1,0,2:T(1,128)} %copy.51), calls=%async_computation.1 | async-start | bytes 16384 | tf_op jit(solution)/shard_map/all_to_all | solution.py:139
  74.6 17.0 %all-to-all-start.2 = ((f32[1,16,16,256]{3,1,0,2:T(8,128)}), f32[1,16,16,256]{3,1,0,2:T(8,128)S(1)}, u32[]{:S(2)}, u32[]{:S(2)}) async-start(f32[1,16,16,256]{3,1,0,2:T(8,128)} %copy.52), calls=%async_computation.2 | async-start | bytes 524288 | tf_op jit(solution)/shard_map/all_to_all | solution.py:140
  78.8 114.8 %all-reduce.3.cloned.1.call-start = ((), (), s32[]{:S(2)}) async-start(), calls=%async_computation.3 | async-start | bytes 262144 | tf_op jit(solution)/shard_map/psum | solution.py:159
  91.7 19.0 %copy-start.7 = (bf16[4,64,256]{2,1,0:T(8,128)(2,1)S(1)}, bf16[4,64,256]{2,1,0:T(8,128)(2,1)}, u32[]{:S(2)}) copy-start(bf16[4,64,256]{2,1,0:T(8,128)(2,1)} %param.34) | copy-start | bytes 393220
  106.8 34.4 %copy-start.2 = (bf16[256,2048]{1,0:T(8,128)(2,1)S(1)}, bf16[256,2048]{1,0:T(8,128)(2,1)}, u32[]{:S(2)}) copy-start(bf16[256,2048]{1,0:T(8,128)(2,1)} %param.36) | copy-start | bytes 3145732
  106.8 20.7 %copy-start.6 = (bf16[16,256]{1,0:T(8,128)(2,1)S(1)}, bf16[16,256]{1,0:T(8,128)(2,1)}, u32[]{:S(2)}) copy-start(bf16[16,256]{1,0:T(8,128)(2,1)} %param.20) | copy-start | bytes 24580
  109.3 84.3 %copy-start.3 = (bf16[2048,256]{1,0:T(8,128)(2,1)S(1)}, bf16[2048,256]{1,0:T(8,128)(2,1)}, u32[]{:S(2)}) copy-start(bf16[2048,256]{1,0:T(8,128)(2,1)} %param.37) | copy-start | bytes 3145732
Sparse Core Ops, SparseCore 0:
  142.3 51.2 all-reduce.2
